TPU v7x, 32 devices: a whole 2x2x4 slice. The times are simulated.
32 devices in a mesh: sp: 8 (over z, x), tp: 4 (over y, core).
Axes of the slice: x: 2, y: 2, z: 4, core: 2. Of those that a mesh axis runs over, the one named last changes fastest.
Arguments:
- resid: bfloat16 [6144, 2048], P(('sp', 'tp')), may hold values from -6 to 6
- queries: bfloat16 [6144, 1024], P('sp', 'tp'), may hold values from -160 to 160
- keys: bfloat16 [6144, 1024], P('sp', 'tp'), may hold values from -6 to 6
- values: bfloat16 [6144, 1024], P('sp', 'tp'), may hold values from -6 to 6
- cum_gate: float32 [6144, 16], P('sp', 'tp'), may hold values from -694 to 0, as said below
- out_weight: bfloat16 [1024, 2048], P('tp'), may hold values from -0.375 to 0.375
- norm_gain: float32 [2048], replicated, may hold values from 0.1 to 1.9
- gate_weight: bfloat16 [2048, 5504], P('sp', 'tp'), may hold values from -0.125 to 0.125
- up_weight: bfloat16 [2048, 5504], P('sp', 'tp'), may hold values from -0.125 to 0.125
- down_weight: bfloat16 [5504, 2048], P('tp', 'sp'), may hold values from -0.078125 to 0.078125
Outputs:
- layer_out: bfloat16 [6144, 2048], P(('sp', 'tp'))
Inputs may be any that keep to these rules, and one draw needn't show every extreme that they name: `cum_gate`: each column is non-increasing along positions and starts at or below zero.
All inputs are finite; a program needn't handle non-finite values.
Results may differ from a plain program's by a relative error of at most 0.01.
Values may be sent and summed in bfloat16 or wider, within the bound.
No kernel may reach another device: no remote copies, remote signals or barrier semaphores. Data moves between devices by JAX's collectives and lax.ppermute only.
A program may use at most 256 MiB of HBM per device.

v0:
```python
import jax
import jax.numpy as jnp
from jax import lax
from jax.sharding import PartitionSpec as P

HEAD_DIM = 64


def rms_norm(mixed, norm_gain):
    scaled = mixed * lax.rsqrt(jnp.mean(mixed * mixed, axis=-1, keepdims=True) + 1e-06) * norm_gain
    return scaled.astype(jnp.bfloat16)


def rounded(term):
    return term.astype(jnp.bfloat16).astype(jnp.float32)


def local(
    resid,
    queries,
    keys,
    values,
    cum_gate,
    out_weight,
    norm_gain,
    gate_weight,
    up_weight,
    down_weight,
):
    rows = queries.shape[0]
    heads_here = cum_gate.shape[1]
    scale = HEAD_DIM ** (-0.5)
    proj_weight = lax.all_gather(out_weight, "tp", axis=0, tiled=True)
    first = lax.axis_index("sp") * rows
    gates_all = lax.all_gather(cum_gate, "sp", axis=0, tiled=True)
    query_heads = queries.reshape(rows, heads_here, HEAD_DIM)
    query_pos = first + jnp.arange(rows, dtype=jnp.int32)
    query_gate = cum_gate.T
    best = jnp.full((heads_here, rows), -1e30, jnp.float32)
    key_piece = lax.all_gather(keys, "sp", axis=0, tiled=True)
    value_piece = lax.all_gather(values, "sp", axis=0, tiled=True)
    count = key_piece.shape[0]
    key_heads = key_piece.reshape(count, heads_here, HEAD_DIM)
    value_heads = value_piece.reshape(count, heads_here, HEAD_DIM)
    key_gate = gates_all.T
    score = (
        jnp.einsum("qhd,khd->hqk", query_heads, key_heads, preferred_element_type=jnp.float32)
        * scale
    )
    score = score + query_gate[:, :, None] - key_gate[:, None, :]
    key_pos = jnp.arange(count, dtype=jnp.int32)
    score = jnp.where(key_pos[None, None, :] <= query_pos[None, :, None], score, -jnp.inf)
    new_best = jnp.maximum(best, jnp.max(score, axis=-1))
    weight = jnp.exp(score - new_best[:, :, None])
    total = jnp.sum(weight, axis=-1)
    numer = jnp.einsum(
        "hqk,khd->hqd", weight.astype(jnp.bfloat16), value_heads, preferred_element_type=jnp.float32
    )
    best, total, numer = (new_best, total, numer)
    attn = (
        (numer / total[:, :, None])
        .transpose(1, 0, 2)
        .reshape(rows, heads_here * HEAD_DIM)
        .astype(jnp.bfloat16)
    )
    groups = lax.axis_size("tp")
    share = rows // groups
    own_rows = lax.all_to_all(attn, "tp", split_axis=0, concat_axis=1, tiled=True)
    group_width = attn.shape[1]
    row_groups = own_rows.reshape(share, groups, group_width)
    weight_groups = proj_weight.reshape(groups, group_width, proj_weight.shape[1])
    terms = jnp.einsum(
        "rgc,gcd->grd", row_groups, weight_groups, preferred_element_type=jnp.float32
    )
    proj = jnp.sum(rounded(terms), axis=0)
    mixed = resid.astype(jnp.float32) + proj
    normed_all = lax.all_gather(rms_norm(mixed, norm_gain), "tp", axis=0, tiled=True)
    gate_sum = jnp.dot(
        normed_all,
        lax.all_gather(gate_weight, "sp", axis=0, tiled=True),
        preferred_element_type=jnp.float32,
    )
    up_sum = jnp.dot(
        normed_all,
        lax.all_gather(up_weight, "sp", axis=0, tiled=True),
        preferred_element_type=jnp.float32,
    )
    hidden = (jax.nn.silu(gate_sum) * up_sum).astype(jnp.bfloat16)
    ffn_part = jnp.dot(
        hidden,
        lax.all_gather(down_weight, "sp", axis=1, tiled=True),
        preferred_element_type=jnp.float32,
    )
    ffn = lax.psum_scatter(
        rounded(ffn_part).astype(jnp.bfloat16), "tp", scatter_dimension=0, tiled=True
    ).astype(jnp.float32)
    return (mixed + 0.5 * ffn).astype(jnp.bfloat16)


def solution(mesh):
    in_specs = (
        P(("sp", "tp"), None),
        P("sp", "tp"),
        P("sp", "tp"),
        P("sp", "tp"),
        P("sp", "tp"),
        P("tp", None),
        P(),
        P("sp", "tp"),
        P("sp", "tp"),
        P("tp", "sp"),
    )
    out_specs = P(("sp", "tp"), None)
    return jax.shard_map(local, mesh=mesh, in_specs=in_specs, out_specs=out_specs, check_vma=False)
```

profile of v0, /device:TPU:0, one launch (start us, length us, event | category | flops | bytes accessed | tf_op | source)
XLA Modules:
  0.0 547.6 jit_solution(295551948475313620)
XLA Ops:
  6.5 0.0 copy-start.2
  6.5 0.0 copy-start.1
  6.5 0.0 all-gather.8.cloned.1.call-start
  6.5 0.7 all-gather.8.cloned.1.call-update
  7.3 0.0 all-gather.10.cloned.1.call-start
  7.3 0.7 all-gather.10.cloned.1.call-update
  8.0 0.0 all-gather.12.cloned.1.call-start
  8.1 0.7 all-gather.12.cloned.1.call-update
  8.7 0.0 all-gather.16.cloned.1.call-start
  8.8 0.5 all-gather.16.cloned.1.call-update
  9.3 0.0 all-gather.14.cloned.1.call-start
  9.4 5.7 %iota_compare_fusion = pred[768,6144]{1,0:T(8,128)(4,1)} fusion(s32[768]{0:T(1024)S(1)} %iota_add_fusion), kind=kLoop, calls=%fused_computation.7 | loop fusion | flops 4718592 | bytes 4721664 | tf_op jit(solution)/shard_map/le | solution.py:52
  15.1 0.0 copy-done.2
  15.1 32.9 %all_gather.25 = f32[6144,4]{0,1:T(4,128)S(1)} all-gather(f32[768,4]{0,1:T(4,128)S(1)} %copy-done.2), channel_id=1, replica_groups=mesh['sp'=8,'tp'=4] {'sp'}, dimensions={0}, use_global_device_ids=true | all-gather | bytes 110592 | tf_op jit(solution)/shard_map/all_gather | solution.py:35
  47.9 0.0 copy-done.1
  48.0 0.9 copy.15
  48.9 23.7 %all-gather.8.cloned.1.call-done = bf16[6144,256]{1,0:T(8,128)(2,1)} async-done(((bf16[768,256]{1,0:T(8,128)(2,1)}), bf16[6144,256]{1,0:T(8,128)(2,1)}) %all-gather.8.cloned.1.call-update) | async-done | bytes 3145744 | tf_op jit(solution)/shard_map/all_gather | solution.py:40
  72.6 3.3 copy.16
  76.0 31.1 %fusion.2 = (f32[4,768]{1,0:T(4,128)S(1)}, f32[4,768,6144]{2,1,0:T(8,128)}) fusion(f32[4,6144]{1,0:T(4,128)S(1)} %bitcast.30, f32[4,768]{1,0:T(4,128)S(1)} %bitcast.34, pred[768,6144]{1,0:T(8,128)(4,1)} %iota_compare_fusion, bf16[768,4,64]{0,2,1:T(8,128)(2,1)} %bitcast.33, bf16[6144,4,64]{0,2,1:T(8,128)(2,1)S(1)} %bitcast.29), kind=kOutput, calls=%fused_computation.4 | convolution fusion | flops 2510287872 | bytes 83877888 | tf_op jit(solution)/shard_map/qhd,khd->hqk/dot_general | solution.py:47
  107.1 26.6 %all-gather.10.cloned.1.call-done = bf16[6144,256]{1,0:T(8,128)(2,1)} async-done(((bf16[768,256]{1,0:T(8,128)(2,1)}), bf16[6144,256]{1,0:T(8,128)(2,1)}) %all-gather.10.cloned.1.call-update) | async-done | bytes 3145744 | tf_op jit(solution)/shard_map/all_gather | solution.py:41
  133.7 3.2 copy.17
  136.9 30.4 %fusion = f32[4,768]{1,0:T(4,128)S(1)} fusion(f32[4,768,6144]{2,1,0:T(8,128)} %get-tuple-element.6, f32[4,768]{1,0:T(4,128)S(1)} %broadcast_maximum_fusion, f32[4,6144]{1,0:T(4,128)S(1)} %bitcast.31, f32[4,768]{1,0:T(4,128)S(1)} %bitcast.35, pred[768,6144]{1,0:T(8,128)(4,1)} %iota_compare_fusion), kind=kLoop, calls=%fused_computation.2 | loop fusion | flops 113243136 | bytes 80351232 | tf_op jit(solution)/shard_map/reduce_sum | solution.py:55
  167.3 31.7 %fusion.12 = bf16[768,4,64]{0,2,1:T(8,128)(2,1)} fusion(bf16[6144,4,64]{0,2,1:T(8,128)(2,1)S(1)} %bitcast.28, f32[4,768,6144]{2,1,0:T(8,128)} %get-tuple-element.6, f32[4,768]{1,0:T(4,128)S(1)} %broadcast_maximum_fusion, f32[4,6144]{1,0:T(4,128)S(1)} %bitcast.32, f32[4,768]{1,0:T(4,128)S(1)} %bitcast.36, pred[768,6144]{1,0:T(8,128)(4,1)} %iota_compare_fusion, ...), kind=kOutput, calls=%fused_computation.18 | convolution fusion | flops 2529558528 | bytes 83890176 | tf_op jit(solution)/shard_map/hqk,khd->hqd/dot_general | solution.py:56
  198.9 1.5 convert_element_type.39
  200.4 0.3 copy.18
  200.8 0.0 copy-start
  200.8 9.9 %all_to_all.13 = bf16[4,192,256]{2,1,0:T(8,128)(2,1)S(1)} all-to-all(bf16[4,192,256]{2,1,0:T(8,128)(2,1)S(1)} %copy.18), channel_id=1, replica_groups=mesh['sp'=8,'tp'=4] {'tp'}, dimensions={0} | all-to-all | bytes 786432 | tf_op jit(solution)/shard_map/all_to_all | solution.py:68
  210.7 0.0 all-gather.12.cloned.1.call-done
  210.7 3.5 convert_reduce_fusion
  214.2 0.0 copy-done
  214.2 0.3 multiply_reduce_fusion
  214.5 0.0 copy-done.3
  214.5 1.1 multiply_convert_fusion.1
  215.6 0.0 all-gather.14.cloned.1.call-update
  215.7 0.0 all-gather.18.cloned.1.call-start
  215.7 0.5 all-gather.18.cloned.1.call-update
  216.2 0.0 all-gather.20.cloned.1.call-start
  216.3 0.7 all-gather.20.cloned.1.call-update
  217.0 0.3 reduce-scatter.2.cloned.1.call-start
  217.2 44.6 %all-gather.16.cloned.1.call-done = bf16[2048,1376]{0,1:T(8,128)(2,1)} async-done(((bf16[256,1376]{0,1:T(8,128)(2,1)}), bf16[2048,1376]{0,1:T(8,128)(2,1)}) %all-gather.16.cloned.1.call-update) | async-done | bytes 5636112 | tf_op jit(solution)/shard_map/all_gather | solution.py:80
  261.9 28.1 %all-gather.14.cloned.1.call-done = bf16[768,2048]{1,0:T(8,128)(2,1)} async-done(((bf16[192,2048]{1,0:T(8,128)(2,1)}), bf16[768,2048]{1,0:T(8,128)(2,1)}) %all-gather.14.cloned.1.call-update) | async-done | bytes 3145744 | tf_op jit(solution)/shard_map/all_gather | solution.py:77
  290.0 10.2 %fusion.19 = f32[768,1376]{0,1:T(8,128)} fusion(bf16[768,2048]{1,0:T(8,128)(2,1)} %all-gather.14.cloned.1.call-done, bf16[2048,1376]{0,1:T(8,128)(2,1)} %all-gather.16.cloned.1.call-done), kind=kOutput, calls=%fused_computation.26 | convolution fusion | flops 4328521728 | bytes 13008896 | tf_op jit(solution)/shard_map/dot_general | solution.py:78
  300.2 83.3 %all-gather.18.cloned.1.call-done = bf16[2048,1376]{0,1:T(8,128)(2,1)} async-done(((bf16[256,1376]{0,1:T(8,128)(2,1)}), bf16[2048,1376]{0,1:T(8,128)(2,1)}) %all-gather.18.cloned.1.call-update) | async-done | bytes 5636112 | tf_op jit(solution)/shard_map/all_gather | solution.py:85
  383.5 91.8 %all-gather.20.cloned.1.call-done = bf16[1376,2048]{1,0:T(8,128)(2,1)} async-done(((bf16[1376,256]{1,0:T(8,128)(2,1)}), bf16[1376,2048]{1,0:T(8,128)(2,1)}) %all-gather.20.cloned.1.call-update) | async-done | bytes 5636112 | tf_op jit(solution)/shard_map/all_gather | solution.py:91
  475.3 26.5 %convolution_convert_fusion.1 = bf16[768,2048]{1,0:T(8,128)(2,1)} fusion(bf16[1376,2048]{1,0:T(8,128)(2,1)} %all-gather.20.cloned.1.call-done, f32[768,1376]{0,1:T(8,128)} %fusion.19, bf16[768,2048]{1,0:T(8,128)(2,1)} %all-gather.14.cloned.1.call-done, bf16[2048,1376]{0,1:T(8,128)(2,1)} %all-gather.18.cloned.1.call-done), kind=kOutput, calls=%fused_computation.11 | convolution fusion | flops 8664956928 | bytes 21790720 | tf_op jit(solution)/shard_map/dot_general | solution.py:89
  501.8 0.0 reduce-scatter.2.cloned.1.call-update
  501.8 36.2 %reduce-scatter.2.cloned.1.call-done = bf16[192,2048]{1,0:T(8,128)(2,1)} async-done(((bf16[768,2048]{1,0:T(8,128)(2,1)}), bf16[192,2048]{1,0:T(8,128)(2,1)}) %reduce-scatter.2.cloned.1.call-update) | async-done | bytes 786448 | tf_op jit(solution)/shard_map/reduce_scatter | solution.py:94
  538.0 2.3 add_convert_fusion
  (4 shorter events, 0.0 us)
Async XLA Ops:
  6.5 8.6 %copy-start.2 = (f32[768,4]{0,1:T(4,128)S(1)}, f32[768,4]{0,1:T(4,128)}, u32[]{:S(2)}) copy-start(f32[768,4]{0,1:T(4,128)} %param.14) | copy-start | bytes 36868
  6.5 41.4 %copy-start.1 = (bf16[768,256]{1,0:T(8,128)(2,1)S(1)}, bf16[768,256]{1,0:T(8,128)(2,1)}, u32[]{:S(2)}) copy-start(bf16[768,256]{1,0:T(8,128)(2,1)} %param.11) | copy-start | bytes 1179652
  6.5 66.1 %all-gather.8.cloned.1.call-start = ((), (), s32[]{:S(2)}) async-start(), calls=%async_computation.2 | async-start | bytes 3538944 | tf_op jit(solution)/shard_map/all_gather | solution.py:40
  7.3 126.4 %all-gather.10.cloned.1.call-start = ((), (), s32[]{:S(2)}) async-start(), calls=%async_computation.3 | async-start | bytes 3538944 | tf_op jit(solution)/shard_map/all_gather | solution.py:41
  8.0 202.7 %all-gather.12.cloned.1.call-start = ((), (), s32[]{:S(2)}) async-start(), calls=%async_computation.4 | async-start | bytes 5242880 | tf_op jit(solution)/shard_map/all_gather | solution.py:33
  8.7 253.1 %all-gather.16.cloned.1.call-start = ((), (), s32[]{:S(2)}) async-start(), calls=%async_computation.6 | async-start | bytes 6340608 | tf_op jit(solution)/shard_map/all_gather | solution.py:80
  9.3 280.7 %all-gather.14.cloned.1.call-start = ((), (), s32[]{:S(2)}) async-start(), calls=%async_computation.5 | async-start | bytes 3932160 | tf_op jit(solution)/shard_map/all_gather | solution.py:77
  200.8 13.4 %copy-start = (bf16[192,2048]{1,0:T(8,128)(2,1)S(1)}, bf16[192,2048]{1,0:T(8,128)(2,1)}, u32[]{:S(2)}) copy-start(bf16[192,2048]{1,0:T(8,128)(2,1)} %param.10) | copy-start | bytes 2359300
  210.7 3.8 copy-start.3
  215.7 167.8 %all-gather.18.cloned.1.call-start = ((), (), s32[]{:S(2)}) async-start(), calls=%async_computation.7 | async-start | bytes 6340608 | tf_op jit(solution)/shard_map/all_gather | solution.py:85
  216.2 259.1 %all-gather.20.cloned.1.call-start = ((), (), s32[]{:S(2)}) async-start(), calls=%async_computation.8 | async-start | bytes 6340608 | tf_op jit(solution)/shard_map/all_gather | solution.py:91
  217.0 321.0 %reduce-scatter.2.cloned.1.call-start = ((), (), s32[]{:S(2)}) async-start(), calls=%async_computation.9 | async-start | bytes 3932160 | tf_op jit(solution)/shard_map/reduce_scatter | solution.py:94
Sparse Core Ops, SparseCore 0:
  9.5 63.0 all-gather.7
  74.8 58.8 all-gather.9
  135.3 33.1 all-gather.11
  170.3 91.5 all-gather.15
  263.3 26.6 all-gather.13
  291.9 91.5 all-gather.17
  385.5 89.7 all-gather.19
  501.9 36.0 reduce-scatter.1
where the time goes:
time: 552 us; the launch traced here: 548 us
  waiting for transfers between devices  338 us (61%)
  matrix products  103 us (19%)
  blocking collectives  42.8 us (8%)
  other arithmetic  39.9 us (7%)
  between operations  14 us (3%)
  local copies, waits for them, and re-layouts  9.28 us (2%)
    all_gather x1, waiting for transfers between devices, local(): lax.all_gather(down_weight, 'sp', axis=1, tiled=True)  91.8 us
    all_gather x1, waiting for transfers between devices, local(): lax.all_gather(up_weight, 'sp', axis=0, tiled=True)  83.3 us
    all_gather x1, waiting for transfers between devices, local(): lax.all_gather(gate_weight, 'sp', axis=0, tiled=True)  44.6 us
    reduce_scatter x1, waiting for transfers between devices, local(): lax.psum_scatter(rounded(ffn_part).astype(jnp.bfloat16), 'tp', scatter_di...  36.2 us
    all_gather x1, blocking collectives, local(): gates_all = lax.all_gather(cum_gate, 'sp', axis=0, tiled=True)  32.9 us
    dot_general x1, matrix products, local(): jnp.einsum('hqk,khd->hqd', weight.astype(jnp.bfloat16), value_heads, pref...  31.7 us
    dot_general x1, matrix products, local(): jnp.einsum('qhd,khd->hqk', query_heads, key_heads, preferred_element_type...  31.1 us
    reduce_sum x1, other arithmetic, local(): total = jnp.sum(weight, axis=-1)  30.4 us
  transfers between devices with their start and end apart: 8, of which 7 were waited for; matrix products, arithmetic and copies ran while one was open for 23% of the time, Pallas kernels for 0%

commit v1 on v0

v1 whole, which is shorter than its diff:
```python
import functools
import math

import jax
import jax.numpy as jnp
from jax import lax
from jax.experimental import pallas as pl
from jax.experimental.pallas import tpu as pltpu
from jax.sharding import Mesh, PartitionSpec as P

HEAD_DIM = 64
LANES = 128
BF = jnp.bfloat16
F32 = jnp.float32


def rms_norm(mixed, norm_gain):
    scaled = mixed * lax.rsqrt(jnp.mean(mixed * mixed, axis=-1, keepdims=True) + 1e-06) * norm_gain
    return scaled.astype(BF)


def rounded(term):
    return term.astype(BF).astype(F32)


def flash_kernel(first_ref, q_ref, k_ref, g_ref, v_ref, o_ref, *, heads, chunk):
    block, width = q_ref.shape
    start = first_ref[0] + pl.program_id(0) * block
    full = start // chunk
    lane = lax.broadcasted_iota(jnp.int32, (block, width), 1)
    glane = lax.broadcasted_iota(jnp.int32, (block, LANES), 1)
    queries = q_ref[...]
    scale = HEAD_DIM ** (-0.5)
    ones = jnp.ones((chunk, LANES), BF)
    outs = []
    for head in range(heads):
        mine = (lane >= head * HEAD_DIM) & (lane < (head + 1) * HEAD_DIM)
        q_part = jnp.where(mine, queries.astype(F32) * scale, 0.0).astype(BF)
        g_mine = (glane >= 3 * head) & (glane < 3 * head + 3)
        g_part = jnp.where(g_mine, -1.0, 0.0).astype(BF)
        q_full = jnp.concatenate([q_part, g_part], axis=1)

        def step(index, carry, masked, q_full=q_full):
            best, acc = carry
            at = pl.multiple_of(index * chunk, chunk)
            k_full = jnp.concatenate([k_ref[pl.ds(at, chunk), :], g_ref[pl.ds(at, chunk), :]], axis=1)
            v_full = jnp.concatenate([v_ref[pl.ds(at, chunk), :], ones], axis=1)
            score = lax.dot_general(q_full, k_full, (((1,), (1,)), ((), ())), preferred_element_type=F32)
            if masked:
                q_pos = start + lax.broadcasted_iota(jnp.int32, score.shape, 0)
                k_pos = at + lax.broadcasted_iota(jnp.int32, score.shape, 1)
                score = jnp.where(k_pos <= q_pos, score, -jnp.inf)
            new_best = jnp.maximum(best, jnp.max(score, axis=-1, keepdims=True))
            weight = jnp.exp(score - new_best).astype(BF)
            acc = acc * jnp.exp(best - new_best) + lax.dot_general(
                weight, v_full, (((1,), (0,)), ((), ())), preferred_element_type=F32
            )
            return new_best, acc

        carry = (jnp.full((block, 1), -1e30, F32), jnp.zeros((block, width + LANES), F32))
        carry = lax.fori_loop(0, full, functools.partial(step, masked=False), carry)
        _, acc = step(full, carry, True)
        outs.append((acc[:, :width] / acc[:, width : width + 1]).astype(BF))
    result = outs[0]
    for head in range(1, heads):
        result = jnp.where(lane >= head * HEAD_DIM, outs[head], result)
    o_ref[...] = result


def flash(first, queries, keys_values, gates, heads):
    rows, width = queries.shape
    count = keys_values.shape[0]
    block = math.gcd(rows, 512)
    elements = heads * rows * count
    return pl.pallas_call(
        functools.partial(flash_kernel, heads=heads, chunk=block),
        grid_spec=pltpu.PrefetchScalarGridSpec(
            num_scalar_prefetch=1,
            grid=(rows // block,),
            in_specs=[
                pl.BlockSpec((block, width), lambda i, s: (i, 0)),
                pl.BlockSpec((count, width), lambda i, s: (0, 0)),
                pl.BlockSpec((count, LANES), lambda i, s: (0, 0)),
                pl.BlockSpec((count, width), lambda i, s: (0, 1)),
            ],
            out_specs=pl.BlockSpec((block, width), lambda i, s: (i, 0)),
        ),
        out_shape=jax.ShapeDtypeStruct((rows, width), BF),
        compiler_params=pltpu.CompilerParams(
            dimension_semantics=("arbitrary",), vmem_limit_bytes=40 * 1024 * 1024
        ),
        cost_estimate=pl.CostEstimate(
            flops=elements * 1024, bytes_accessed=4 * count * width * 2, transcendentals=elements
        ),
    )(first, queries, keys_values, gates, keys_values)


def gate_terms(gates):
    high = lax.reduce_precision(gates, 8, 7)
    rest = gates - high
    mid = lax.reduce_precision(rest, 8, 7)
    low = rest - mid
    count, heads = gates.shape
    terms = jnp.stack([high, mid, low], axis=-1).reshape(count, 3 * heads).astype(BF)
    return jnp.pad(terms, ((0, 0), (0, LANES - 3 * heads)))


def pair_exchange(array, axis, concat_axis, size):
    half = array.shape[axis] // size
    halves = [lax.slice_in_dim(array, i * half, (i + 1) * half, axis=axis) for i in range(size)]
    odd = lax.axis_index("x") == 1
    mine = jnp.where(odd, halves[1], halves[0])
    other = jnp.where(odd, halves[0], halves[1])
    got = lax.ppermute(other, "x", [(0, 1), (1, 0)])
    return jnp.concatenate([jnp.where(odd, got, mine), jnp.where(odd, mine, got)], axis=concat_axis)


def swap(array, hop):
    axis, mask = hop
    return lax.ppermute(array, axis, [(i, i ^ mask) for i in range(lax.axis_size(axis))])


def hops_of():
    tp_size = lax.axis_size("tp")
    return [("tp", 1 << i) for i in range(tp_size.bit_length() - 1)] + [("x", 1)]


def orders(count):
    links = list(range(1, count))
    return links, links[::-1]


def gather_rows(own):
    hops = hops_of()
    half = own.shape[1] // 2
    parts = []
    for order, columns in zip(orders(len(hops)), (own[:, :half], own[:, half:])):
        block = columns.reshape((1,) * len(hops) + columns.shape)
        parts.append([block, order])
    for level in range(len(hops) - 1):
        for part in parts:
            at = part[1][level]
            part[0] = jnp.concatenate([part[0], swap(part[0], hops[at])], axis=at)
    both = []
    for block, _ in parts:
        block = jnp.concatenate([block, swap(block, hops[0])], axis=0)
        both.append(block.reshape(-1, half))
    return jnp.concatenate(both, axis=1)


def add(a, b):
    return a.astype(F32) + b.astype(F32)


def scatter_rows(halves, rows):
    hops = hops_of()
    pick = lambda a, at, i: lax.slice_in_dim(a, i, i + 1, axis=at)
    results = []
    parts = []
    for order, columns in zip(orders(len(hops)), halves):
        block = columns.reshape((2,) * len(hops) + (rows, columns.shape[1]))
        parts.append([add(pick(block, 0, 0), swap(pick(block, 0, 1), hops[0])).astype(BF), order])
    for level in range(len(hops) - 1):
        for part in parts:
            at = part[1][level]
            total = add(pick(part[0], at, 0), swap(pick(part[0], at, 1), hops[at]))
            part[0] = total if level == len(hops) - 2 else total.astype(BF)
    return [p[0].reshape(rows, -1) for p in parts]


def gather_groups(piece):
    count = lax.axis_size("tp")
    return [piece] + [swap(piece, ("tp", k)) for k in range(1, count)]


def local(
    resid, queries, keys, values, cum_gate, out_weight, norm_gain, gate_weight, up_weight, down_weight,
    *, pair,
):
    groups = lax.axis_size("tp")
    heads_here = cum_gate.shape[1] // pair
    columns = down_weight.shape[1]
    down_half = pair_exchange(down_weight, 0, 1, pair)
    down_half, stacked = lax.optimization_barrier((down_half, jnp.stack([keys, values, queries])))
    down_first = lax.all_gather(down_half[:, :columns], "z", axis=1, tiled=True)
    packed = lax.all_to_all(stacked, "x", split_axis=2, concat_axis=1, tiled=True)
    query_local = packed[2]
    block_rows, width = query_local.shape
    kv_local = jnp.concatenate([packed[0], packed[1]], axis=1)
    kv_local, down_first = lax.optimization_barrier((kv_local, down_first))
    kv_all = lax.all_gather(kv_local, "z", axis=0, tiled=True)
    gates_all = lax.all_gather(cum_gate, ("z", "x"), axis=0, tiled=True)
    gates_mine = lax.dynamic_slice_in_dim(gates_all, lax.axis_index("x") * heads_here, heads_here, axis=1)
    terms_gate = gate_terms(gates_mine)
    proj_pieces = gather_groups(out_weight)
    up_half = pair_exchange(up_weight, 1, 0, pair)
    gate_half = pair_exchange(gate_weight, 1, 0, pair)
    kv_all, terms_gate, gate_half, up_half, down_half = lax.optimization_barrier(
        (kv_all, terms_gate, gate_half, up_half, down_half)
    )
    gate_all = lax.all_gather(gate_half, "z", axis=0, tiled=True)
    up_all = lax.all_gather(up_half, "z", axis=0, tiled=True)
    down_parts = [down_first, lax.all_gather(down_half[:, columns:], "z", axis=1, tiled=True)]

    lane_pad = -width % LANES
    if lane_pad:
        query_local, key_all, value_all = (
            jnp.pad(a, ((0, 0), (0, lane_pad))) for a in (query_local, kv_all[:, :width], kv_all[:, width:])
        )
        kv_all = jnp.concatenate([key_all, value_all], axis=1)
    first = (lax.axis_index("z") * block_rows).astype(jnp.int32).reshape(1)
    attn = flash(first, query_local, kv_all, terms_gate, heads_here)[:, :width]

    own_rows = lax.all_to_all(attn, ("x", "tp"), split_axis=0, concat_axis=1, tiled=True)
    share = own_rows.shape[0]
    row_groups = own_rows.reshape(share, pair, groups, width)
    mixed = resid.astype(F32)
    for k, piece in enumerate(proj_pieces):
        index = lax.axis_index("tp") ^ k
        rows = lax.dynamic_index_in_dim(row_groups, index, axis=2, keepdims=False).reshape(share, pair * width)
        mixed = mixed + rounded(jnp.dot(rows, piece, preferred_element_type=F32))
    normed_all = gather_rows(rms_norm(mixed, norm_gain))
    gate_sum = jnp.dot(normed_all, gate_all, preferred_element_type=F32)
    up_sum = jnp.dot(normed_all, up_all, preferred_element_type=F32)
    hidden = (jax.nn.silu(gate_sum) * up_sum).astype(BF)
    halves = [jnp.dot(hidden, part, preferred_element_type=F32).astype(BF) for part in down_parts]
    sums = scatter_rows(halves, share)
    starts = range(0, sums[0].shape[1], columns)
    ffn = jnp.concatenate([part[:, i : i + columns] for i in starts for part in sums], axis=1)
    return (mixed + 0.5 * ffn).astype(BF)


def solution(mesh):
    sp, tp = mesh.shape["sp"], mesh.shape["tp"]
    pair = 2
    split = Mesh(mesh.devices.reshape(sp // pair, pair, tp), ("z", "x", "tp"))
    seq = ("z", "x")
    in_specs = (
        P(("z", "x", "tp"), None),
        P(seq, "tp"),
        P(seq, "tp"),
        P(seq, "tp"),
        P(seq, "tp"),
        P("tp", None),
        P(),
        P(seq, "tp"),
        P(seq, "tp"),
        P("tp", seq),
    )
    out_specs = P(("z", "x", "tp"), None)
    return jax.shard_map(
        functools.partial(local, pair=pair), mesh=split, in_specs=in_specs, out_specs=out_specs, check_vma=False
    )
```

time: 552 us -> 333 us (0.60)
  waiting for transfers between devices: 338 us -> 152 us
  matrix products: 103 us -> 33.2 us
  starting transfers between devices: 0.48 us -> 24.4 us
  blocking collectives: 42.8 us -> 61.5 us
  other arithmetic: 39.9 us -> 22.6 us
  Pallas kernels: 0 us -> 12.7 us
    all_gather x7 -> x5, waiting for transfers between devices: 298 us -> 65.9 us  [the longest x1 20.9 us: local(): lax.all_gather(down_half[:, columns:], 'z', axis=1, tiled=True)]
    dot_general x5 -> x8, matrix products: 103 us -> 33.2 us  [the longest x1 10.2 us: local(): gate_sum = jnp.dot(normed_all, gate_all, preferred_element_type=F32)]
    ppermute x0 -> x18, waiting for transfers between devices: none -> 55.8 us  [the longest x15 48.9 us: swap(): lax.ppermute(array, axis, [(i, i ^ mask) for i in range(lax.axis_size(axi...]
    reduce_scatter x1 -> x0, waiting for transfers between devices: 36.2 us -> none  [local(): lax.psum_scatter(rounded(ffn_part).astype(jnp.bfloat16), 'tp', scatter_di...]
    reduce_sum x2 -> x0, other arithmetic: 30.7 us -> none  [the longest x1 30.4 us: local(): total = jnp.sum(weight, axis=-1)]
    all_to_all x0 -> x1, waiting for transfers between devices: none -> 30.5 us  [local(): lax.all_to_all(attn, ('x', 'tp'), split_axis=0, concat_axis=1, tiled=True)]
    ppermute x0 -> x18, starting transfers between devices: none -> 20 us  [the longest x15 14.9 us: swap(): lax.ppermute(array, axis, [(i, i ^ mask) for i in range(lax.axis_size(axi...]
    pallas_call x0 -> x1, Pallas kernels: none -> 12.7 us  [flash(): pl.pallas_call(functools.partial(flash_kernel, heads=heads, chunk=block),...]
  transfers between devices with their start and end apart: 8 -> 24, of which waited for: 7 -> 13; matrix products, arithmetic and copies ran while one was open for 23% -> 18% of each run, Pallas kernels for 0% -> 4%
where the time goes in v1:
time: 333 us; the launch traced here: 332 us
  waiting for transfers between devices  152 us (46%)
  blocking collectives  61.5 us (18%)
  matrix products  33.2 us (10%)
  starting transfers between devices  24.4 us (7%)
  other arithmetic  22.6 us (7%)
  between operations  13.7 us (4%)
  Pallas kernels  12.7 us (4%)
  local copies, waits for them, and re-layouts  11.5 us (3%)
    ppermute x15, waiting for transfers between devices, swap(): lax.ppermute(array, axis, [(i, i ^ mask) for i in range(lax.axis_size(axi...  48.9 us
    all_gather x1, blocking collectives, local(): gates_all = lax.all_gather(cum_gate, ('z', 'x'), axis=0, tiled=True)  40.1 us
    all_to_all x1, waiting for transfers between devices, local(): lax.all_to_all(attn, ('x', 'tp'), split_axis=0, concat_axis=1, tiled=True)  30.5 us
    all_to_all x1, blocking collectives, local(): lax.all_to_all(stacked, 'x', split_axis=2, concat_axis=1, tiled=True)  21.4 us
    all_gather x1, waiting for transfers between devices, local(): lax.all_gather(down_half[:, columns:], 'z', axis=1, tiled=True)  20.9 us
    all_gather x1, waiting for transfers between devices, local(): up_all = lax.all_gather(up_half, 'z', axis=0, tiled=True)  18.8 us
    ppermute x15, starting transfers between devices, swap(): lax.ppermute(array, axis, [(i, i ^ mask) for i in range(lax.axis_size(axi...  14.9 us
    all_gather x1, waiting for transfers between devices, local(): kv_all = lax.all_gather(kv_local, 'z', axis=0, tiled=True)  14.4 us
  transfers between devices with their start and end apart: 24, of which 13 were waited for; matrix products, arithmetic and copies ran while one was open for 18% of the time, Pallas kernels for 4%

profile of v1, /device:TPU:0, one launch (start us, length us, event | category | flops | bytes accessed | tf_op | source)
XLA Modules:
  0.0 332.0 jit_solution(11090359744703380088)
XLA Ops:
  6.5 1.2 broadcast_select_fusion.11
  7.7 3.0 collective-permute-start
  10.8 1.4 pad_maximum_fusion.9
  12.1 6.9 %collective-permute-done = bf16[688,256]{1,0:T(8,128)(2,1)S(1)} collective-permute-done((bf16[688,256]{1,0:T(8,128)(2,1)S(1)}, bf16[688,256]{1,0:T(8,128)(2,1)S(1)}, u32[]{:S(2)}, u32[]{:S(2)}) %collective-permute-start) | collective-permute-done | bytes 352288 | tf_op jit(solution)/shard_map/ppermute | solution.py:114
  20.9 1.2 copy.33
  22.0 21.4 %all_to_all.31 = bf16[3,768,256]{1,0,2:T(4,128)(2,1)S(1)} all-to-all(bf16[3,768,256]{1,0,2:T(4,128)(2,1)S(1)} %copy.33), channel_id=1, replica_groups=mesh['z'=4,'x'=2,'tp'=4] {'x'}, dimensions={2} | all-to-all | bytes 2359296 | tf_op jit(solution)/shard_map/all_to_all | solution.py:186
  43.5 1.2 copy.34
  45.7 11.8 %all-gather.6.cloned.1.call-done = bf16[688,1024]{1,0:T(8,128)(2,1)} async-done(((bf16[688,256]{1,0:T(8,128)(2,1)}), bf16[688,1024]{1,0:T(8,128)(2,1)}) %all-gather.6.cloned.1.call-update) | async-done | bytes 1409040 | tf_op jit(solution)/shard_map/all_gather | solution.py:185
  58.4 1.5 collective-permute-start.2
  61.2 40.1 %all_gather.20 = f32[6144,4]{0,1:T(4,128)S(1)} all-gather(f32[768,4]{0,1:T(4,128)S(1)} %copy-done.13), channel_id=1, replica_groups=mesh['z'=4,'x'=2,'tp'=4] {'z','x'}, dimensions={0}, use_global_device_ids=true | all-gather | bytes 110592 | tf_op jit(solution)/shard_map/all_gather | solution.py:192
  103.6 1.1 broadcast_select_fusion.1
  104.7 1.0 broadcast_select_fusion.5
  105.8 1.2 pad_maximum_fusion.14
  107.0 14.4 %all-gather.8.cloned.1.call-done.k_ref.v_ref = bf16[6144,256]{1,0:T(8,128)(2,1)} async-done(((bf16[1536,256]{1,0:T(8,128)(2,1)}), bf16[6144,256]{1,0:T(8,128)(2,1)}) %all-gather.8.cloned.1.call-update) | async-done | bytes 3145744 | tf_op jit(solution)/shard_map/all_gather | solution.py:191
  121.4 1.5 collective-permute-start.4
  122.9 1.9 copy-done
  124.8 12.7 %shard_map.100 = bf16[1536,128]{1,0:T(8,128)(2,1)} custom-call(s32[1]{0:T(128)} %bitcast.first_ref, bf16[1536,128]{1,0:T(8,128)(2,1)S(1)} %bitcast.73, bf16[6144,256]{1,0:T(8,128)(2,1)S(1)} %copy-done, bf16[6144,128]{1,0:T(8,128)(2,1)S(1)} %pad.4.g_ref, bf16[6144,256]{1,0:T(8,128)(2,1)S(1)} %copy-done), custom_call_target="tpu_custom_call" | custom-call | flops 19327352832 | bytes 6291456 | tf_op jit(solution)/shard_map/pallas_call | solution.py:75
  137.5 4.1 %all-to-all-start.1 = ((bf16[8,192,128]{2,1,0:T(8,128)(2,1)}), bf16[8,192,128]{2,1,0:T(8,128)(2,1)S(1)}, u32[]{:S(2)}, u32[]{:S(2)}) async-start(bf16[8,192,128]{2,1,0:T(8,128)(2,1)} %bitcast.12), calls=%async_computation.1 | async-start | bytes 786432 | tf_op jit(solution)/shard_map/all_to_all | solution.py:214
  142.4 30.5 %all-to-all-done.1 = bf16[8,192,128]{2,1,0:T(8,128)(2,1)S(1)} async-done(((bf16[8,192,128]{2,1,0:T(8,128)(2,1)}), bf16[8,192,128]{2,1,0:T(8,128)(2,1)S(1)}, u32[]{:S(2)}, u32[]{:S(2)}) %all-to-all-start.1) | async-done | bytes 393248 | tf_op jit(solution)/shard_map/all_to_all | solution.py:214
  173.4 1.6 fusion.5
  175.0 1.7 fusion.4
  177.1 1.8 multiply_reduce_fusion
  179.2 1.5 collective-permute-start.6
  180.8 1.6 collective-permute-start.9
  182.4 7.6 %collective-permute-done.6 = bf16[1,1,1,192,1024]{4,3,2,1,0:T(8,128)(2,1)S(1)} collective-permute-done((bf16[1,1,1,192,1024]{4,3,2,1,0:T(8,128)(2,1)S(1)}, bf16[1,1,1,192,1024]{4,3,2,1,0:T(8,128)(2,1)S(1)}, u32[]{:S(2)}, u32[]{:S(2)}) %collective-permute-start.6) | collective-permute-done | bytes 393248 | tf_op jit(solution)/shard_map/ppermute | solution.py:120
  190.1 1.6 collective-permute-start.7
  191.8 1.6 collective-permute-start.10
  193.4 15.0 %collective-permute-done.7 = bf16[1,2,1,192,1024]{4,3,2,1,0:T(8,128)(2,1)S(1)} collective-permute-done((bf16[1,2,1,192,1024]{4,3,2,1,0:T(8,128)(2,1)S(1)}, bf16[1,2,1,192,1024]{4,3,2,1,0:T(8,128)(2,1)S(1)}, u32[]{:S(2)}, u32[]{:S(2)}) %collective-permute-start.7) | collective-permute-done | bytes 786464 | tf_op jit(solution)/shard_map/ppermute | solution.py:120
  208.4 1.4 pad_maximum_fusion.7
  209.9 1.3 pad_maximum_fusion.8
  213.6 3.1 pad_maximum_fusion.3
  216.7 3.1 pad_maximum_fusion.4
  219.8 10.2 %fusion.1 = f32[1536,688]{0,1:T(8,128)} fusion(bf16[2048,688]{0,1:T(8,128)(2,1)} %all-gather.10.cloned.1.call-done, bf16[1536,1024]{1,0:T(8,128)(2,1)} %bitcast.80, bf16[1536,1024]{1,0:T(8,128)(2,1)} %bitcast.78), kind=kOutput, calls=%fused_computation.3 | convolution fusion | flops 4341104640 | bytes 13336576 | tf_op jit(solution)/shard_map/dot_general | solution.py:223
  230.0 18.8 %all-gather.12.cloned.1.call-done = bf16[2048,688]{0,1:T(8,128)(2,1)} async-done(((bf16[512,688]{0,1:T(8,128)(2,1)}), bf16[2048,688]{0,1:T(8,128)(2,1)}) %all-gather.12.cloned.1.call-update) | async-done | bytes 2818064 | tf_op jit(solution)/shard_map/all_gather | solution.py:202
  248.8 9.7 %multiply_convert_fusion = bf16[1536,688]{0,1:T(8,128)(2,1)S(1)} fusion(f32[1536,688]{0,1:T(8,128)} %fusion.1, bf16[2048,688]{0,1:T(8,128)(2,1)} %all-gather.12.cloned.1.call-done, bf16[1536,1024]{1,0:T(8,128)(2,1)} %bitcast.81, bf16[1536,1024]{1,0:T(8,128)(2,1)} %bitcast.79), kind=kOutput, calls=%fused_computation.1 | convolution fusion | flops 4347445248 | bytes 15450112 | tf_op jit(solution)/shard_map/dot_general | solution.py:224
  258.5 3.1 convolution_convert_fusion.1
  261.7 1.5 fusion.27
  263.1 20.9 %all-gather.14.cloned.1.call-done = bf16[688,1024]{1,0:T(8,128)(2,1)} async-done(((bf16[688,256]{1,0:T(8,128)(2,1)}), bf16[688,1024]{1,0:T(8,128)(2,1)}) %all-gather.14.cloned.1.call-update) | async-done | bytes 1409040 | tf_op jit(solution)/shard_map/all_gather | solution.py:203
  284.0 4.6 %convolution_convert_fusion = bf16[1536,1024]{1,0:T(8,128)(2,1)S(1)} fusion(bf16[1536,688]{0,1:T(8,128)(2,1)} %copy-done.16, bf16[688,1024]{1,0:T(8,128)(2,1)} %all-gather.14.cloned.1.call-done), kind=kOutput, calls=%fused_computation.4 | convolution fusion | flops 2165833728 | bytes 6668288 | tf_op jit(solution)/shard_map/dot_general | solution.py:226
  289.1 2.1 fusion.3
  291.2 1.5 collective-permute-start.13
  293.5 1.5 collective-permute-start.16
  295.1 16.2 %collective-permute-done.13 = bf16[1,1,2,192,1024]{4,3,2,1,0:T(8,128)(2,1)S(1)} collective-permute-done((bf16[1,1,2,192,1024]{4,3,2,1,0:T(8,128)(2,1)S(1)}, bf16[1,1,2,192,1024]{4,3,2,1,0:T(8,128)(2,1)S(1)}, u32[]{:S(2)}, u32[]{:S(2)}) %collective-permute-start.13) | collective-permute-done | bytes 786464 | tf_op jit(solution)/shard_map/ppermute | solution.py:120
  311.6 1.5 collective-permute-start.14
  313.6 1.4 collective-permute-start.17
  315.0 7.3 %collective-permute-done.14 = bf16[1,1,1,192,1024]{4,3,2,1,0:T(8,128)(2,1)S(1)} collective-permute-done((bf16[1,1,1,192,1024]{4,3,2,1,0:T(8,128)(2,1)S(1)}, bf16[1,1,1,192,1024]{4,3,2,1,0:T(8,128)(2,1)S(1)}, u32[]{:S(2)}, u32[]{:S(2)}) %collective-permute-start.14) | collective-permute-done | bytes 393248 | tf_op jit(solution)/shard_map/ppermute | solution.py:120
  322.4 1.6 collective-permute-done.17
  324.3 1.1 add_convert_fusion
  (106 shorter events, 14.2 us)
Async XLA Ops:
  6.5 51.0 %all-gather.6.cloned.1.call-start = ((), (), s32[]{:S(2)}) async-start(), calls=%async_computation.2 | async-start | bytes 1761280 | tf_op jit(solution)/shard_map/all_gather | solution.py:185
  6.5 12.5 %copy-start.4 = (bf16[1376,256]{1,0:T(8,128)(2,1)S(1)}, bf16[1376,256]{1,0:T(8,128)(2,1)}, u32[]{:S(2)}) copy-start(bf16[1376,256]{1,0:T(8,128)(2,1)} %param.19) | copy-start | bytes 2113540
  7.7 11.3 %collective-permute-start = (bf16[688,256]{1,0:T(8,128)(2,1)S(1)}, bf16[688,256]{1,0:T(8,128)(2,1)S(1)}, u32[]{:S(2)}, u32[]{:S(2)}) collective-permute-start(bf16[688,256]{1,0:T(8,128)(2,1)S(1)} %broadcast_select_fusion.11), channel_id=1, source_target_pairs={{0,4},{4,0},{1,5},{5,1},{2,6},{6,2},{3,7},{7,3},{8,12},{12,8},{9,1... | collective-permute-start | bytes 1056776 | tf_op jit(solution)/shard_map/ppermute | solution.py:114
  19.1 0.9 copy-start.9
  20.8 100.6 %all-gather.8.cloned.1.call-start = ((), (), s32[]{:S(2)}) async-start(), calls=%async_computation.3 | async-start | bytes 3932160 | tf_op jit(solution)/shard_map/all_gather | solution.py:191
  44.7 12.9 %copy-start.5 = (bf16[256,1376]{0,1:T(8,128)(2,1)S(1)}, bf16[256,1376]{0,1:T(8,128)(2,1)}, u32[]{:S(2)}) copy-start(bf16[256,1376]{0,1:T(8,128)(2,1)} %param.18) | copy-start | bytes 2113540
  44.7 15.1 %copy-start.7 = (bf16[256,1376]{0,1:T(8,128)(2,1)S(1)}, bf16[256,1376]{0,1:T(8,128)(2,1)}, u32[]{:S(2)}) copy-start(bf16[256,1376]{0,1:T(8,128)(2,1)} %param.17) | copy-start | bytes 2113540
  45.7 15.5 %copy-start.13 = (f32[768,4]{0,1:T(4,128)S(1)}, f32[768,4]{0,1:T(4,128)}, u32[]{:S(2)}) copy-start(f32[768,4]{0,1:T(4,128)} %param.14) | copy-start | bytes 36868
  57.5 162.2 %all-gather.10.cloned.1.call-start = ((), (), s32[]{:S(2)}) async-start(), calls=%async_computation.4 | async-start | bytes 3522560 | tf_op jit(solution)/shard_map/all_gather | solution.py:201
  58.4 44.4 %collective-permute-start.2 = (bf16[256,688]{0,1:T(8,128)(2,1)}, bf16[256,688]{0,1:T(8,128)(2,1)}, u32[]{:S(2)}, u32[]{:S(2)}) collective-permute-start(bf16[256,688]{0,1:T(8,128)(2,1)} %broadcast_select_fusion.3), channel_id=1, source_target_pairs={{0,4},{4,0},{1,5},{5,1},{2,6},{6,2},{3,7},{7,3},{8,12},{12,8},{9,1... | collective-permute-start | bytes 1056776 | tf_op jit(solution)/shard_map/ppermute | solution.py:114
  60.6 44.0 %collective-permute-start.1 = (bf16[256,688]{0,1:T(8,128)(2,1)}, bf16[256,688]{0,1:T(8,128)(2,1)}, u32[]{:S(2)}, u32[]{:S(2)}) collective-permute-start(bf16[256,688]{0,1:T(8,128)(2,1)} %broadcast_select_fusion.7), channel_id=1, source_target_pairs={{0,4},{4,0},{1,5},{5,1},{2,6},{6,2},{3,7},{7,3},{8,12},{12,8},{9,1... | collective-permute-start | bytes 1056776 | tf_op jit(solution)/shard_map/ppermute | solution.py:114
  102.5 1.1 copy-start.6
  102.8 1.9 copy-start.8
  105.7 15.7 %copy-start.11 = (bf16[256,2048]{1,0:T(8,128)(2,1)S(1)}, bf16[256,2048]{1,0:T(8,128)(2,1)}, u32[]{:S(2)}) copy-start(bf16[256,2048]{1,0:T(8,128)(2,1)} %param.15) | copy-start | bytes 3145732
  121.4 52.0 %collective-permute-start.4 = (bf16[256,2048]{1,0:T(8,128)(2,1)S(1)}, bf16[256,2048]{1,0:T(8,128)(2,1)}, u32[]{:S(2)}, u32[]{:S(2)}) collective-permute-start(bf16[256,2048]{1,0:T(8,128)(2,1)S(1)} %copy-done.11), channel_id=1, source_target_pairs={{0,2},{1,3},{2,0},{3,1},{4,6},{5,7},{6,4},{7,5},{8,10},{9,11},{10,... | collective-permute-start | bytes 3145736 | tf_op jit(solution)/shard_map/ppermute | solution.py:120
  122.9 52.1 %collective-permute-start.5 = (bf16[256,2048]{1,0:T(8,128)(2,1)S(1)}, bf16[256,2048]{1,0:T(8,128)(2,1)}, u32[]{:S(2)}, u32[]{:S(2)}) collective-permute-start(bf16[256,2048]{1,0:T(8,128)(2,1)S(1)} %copy-done.11), channel_id=1, source_target_pairs={{0,3},{1,2},{2,1},{3,0},{4,7},{5,6},{6,5},{7,4},{8,11},{9,10},{10,... | collective-permute-start | bytes 3145736 | tf_op jit(solution)/shard_map/ppermute | solution.py:120
  122.9 1.9 copy-start
  137.5 35.4 %all-to-all-start.1 = ((bf16[8,192,128]{2,1,0:T(8,128)(2,1)}), bf16[8,192,128]{2,1,0:T(8,128)(2,1)S(1)}, u32[]{:S(2)}, u32[]{:S(2)}) async-start(bf16[8,192,128]{2,1,0:T(8,128)(2,1)} %bitcast.12), calls=%async_computation.1 | async-start | bytes 786432 | tf_op jit(solution)/shard_map/all_to_all | solution.py:214
  141.6 107.2 %all-gather.12.cloned.1.call-start = ((), (), s32[]{:S(2)}) async-start(), calls=%async_computation.5 | async-start | bytes 3522560 | tf_op jit(solution)/shard_map/all_gather | solution.py:202
  141.6 35.4 %collective-permute-start.3 = (bf16[256,2048]{1,0:T(8,128)(2,1)S(1)}, bf16[256,2048]{1,0:T(8,128)(2,1)}, u32[]{:S(2)}, u32[]{:S(2)}) collective-permute-start(bf16[256,2048]{1,0:T(8,128)(2,1)S(1)} %copy-done.11), channel_id=1, source_target_pairs={{0,1},{1,0},{2,3},{3,2},{4,5},{5,4},{6,7},{7,6},{8,9},{9,8},{10,11... | collective-permute-start | bytes 3145736 | tf_op jit(solution)/shard_map/ppermute | solution.py:120
  142.2 141.8 %all-gather.14.cloned.1.call-start = ((), (), s32[]{:S(2)}) async-start(), calls=%async_computation.6 | async-start | bytes 1761280 | tf_op jit(solution)/shard_map/all_gather | solution.py:203
  175.0 1.7 copy-start.12
  177.1 1.9 copy-start.14
  179.2 10.8 %collective-permute-start.6 = (bf16[1,1,1,192,1024]{4,3,2,1,0:T(8,128)(2,1)S(1)}, bf16[1,1,1,192,1024]{4,3,2,1,0:T(8,128)(2,1)S(1)}, u32[]{:S(2)}, u32[]{:S(2)}) collective-permute-start(bf16[1,1,1,192,1024]{4,3,2,1,0:T(8,128)(2,1)S(1)} %get-tuple-element.36), channel_id=1, source_target_pairs={{0,2},{1,3},{2,0},{3,1},{4,6},{5,7},{6,4},{7,5},{8,10},{9,11},{10,... | collective-permute-start | bytes 1179656 | tf_op jit(solution)/shard_map/ppermute | solution.py:120
  180.8 10.9 %collective-permute-start.9 = (bf16[1,1,1,192,1024]{4,3,2,1,0:T(8,128)(2,1)S(1)}, bf16[1,1,1,192,1024]{4,3,2,1,0:T(8,128)(2,1)S(1)}, u32[]{:S(2)}, u32[]{:S(2)}) collective-permute-start(bf16[1,1,1,192,1024]{4,3,2,1,0:T(8,128)(2,1)S(1)} %get-tuple-element.37), channel_id=1, source_target_pairs={{0,4},{4,0},{1,5},{5,1},{2,6},{6,2},{3,7},{7,3},{8,12},{12,8},{9,1... | collective-permute-start | bytes 1179656 | tf_op jit(solution)/shard_map/ppermute | solution.py:120
  190.1 18.3 %collective-permute-start.7 = (bf16[1,2,1,192,1024]{4,3,2,1,0:T(8,128)(2,1)S(1)}, bf16[1,2,1,192,1024]{4,3,2,1,0:T(8,128)(2,1)S(1)}, u32[]{:S(2)}, u32[]{:S(2)}) collective-permute-start(bf16[1,2,1,192,1024]{4,3,2,1,0:T(8,128)(2,1)S(1)} %pad_maximum_fusion.11), channel_id=1, source_target_pairs={{0,4},{4,0},{1,5},{5,1},{2,6},{6,2},{3,7},{7,3},{8,12},{12,8},{9,1... | collective-permute-start | bytes 2359304 | tf_op jit(solution)/shard_map/ppermute | solution.py:120
  191.8 18.1 %collective-permute-start.10 = (bf16[1,1,2,192,1024]{4,3,2,1,0:T(8,128)(2,1)S(1)}, bf16[1,1,2,192,1024]{4,3,2,1,0:T(8,128)(2,1)S(1)}, u32[]{:S(2)}, u32[]{:S(2)}) collective-permute-start(bf16[1,1,2,192,1024]{4,3,2,1,0:T(8,128)(2,1)S(1)} %pad_maximum_fusion.12), channel_id=1, source_target_pairs={{0,2},{1,3},{2,0},{3,1},{4,6},{5,7},{6,4},{7,5},{8,10},{9,11},{10,... | collective-permute-start | bytes 2359304 | tf_op jit(solution)/shard_map/ppermute | solution.py:120
  208.4 1.4 copy-start.3
  209.9 1.9 copy-start.10
  209.9 3.8 %collective-permute-start.8 = (bf16[1,2,2,192,1024]{4,3,2,1,0:T(8,128)(2,1)}, bf16[1,2,2,192,1024]{4,3,2,1,0:T(8,128)(2,1)}, u32[]{:S(2)}, u32[]{:S(2)}) collective-permute-start(bf16[1,2,2,192,1024]{4,3,2,1,0:T(8,128)(2,1)} %pad_maximum_fusion.7), channel_id=1, source_target_pairs={{0,1},{1,0},{2,3},{3,2},{4,5},{5,4},{6,7},{7,6},{8,9},{9,8},{10,11... | collective-permute-start | bytes 4718600 | tf_op jit(solution)/shard_map/ppermute | solution.py:120
  209.9 1.4 copy-start.1
  211.3 5.4 %collective-permute-start.11 = (bf16[1,2,2,192,1024]{4,3,2,1,0:T(8,128)(2,1)}, bf16[1,2,2,192,1024]{4,3,2,1,0:T(8,128)(2,1)}, u32[]{:S(2)}, u32[]{:S(2)}) collective-permute-start(bf16[1,2,2,192,1024]{4,3,2,1,0:T(8,128)(2,1)} %pad_maximum_fusion.8), channel_id=1, source_target_pairs={{0,1},{1,0},{2,3},{3,2},{4,5},{5,4},{6,7},{7,6},{8,9},{9,8},{10,11... | collective-permute-start | bytes 4718600 | tf_op jit(solution)/shard_map/ppermute | solution.py:120
  212.6 4.1 %copy-start.2 = (bf16[1,1,2,192,1024]{4,3,2,1,0:T(8,128)(2,1)S(1)}, bf16[1,1,2,192,1024]{4,3,2,1,0:T(8,128)(2,1)}, u32[]{:S(2)}) copy-start(bf16[1,1,2,192,1024]{4,3,2,1,0:T(8,128)(2,1)} %copy-done.1) | copy-start | bytes 2359300
  230.0 28.5 %copy-start.15 = (bf16[688,1024]{1,0:T(8,128)(2,1)S(1)}, bf16[688,1024]{1,0:T(8,128)(2,1)}, u32[]{:S(2)}) copy-start(bf16[688,1024]{1,0:T(8,128)(2,1)} %all-gather.6.cloned.1.call-done) | copy-start | bytes 4227076
  258.5 3.2 copy-start.16
  263.1 26.0 %collective-permute-start.12 = (bf16[1,2,2,192,1024]{4,3,2,1,0:T(8,128)(2,1)}, bf16[1,2,2,192,1024]{4,3,2,1,0:T(8,128)(2,1)}, u32[]{:S(2)}, u32[]{:S(2)}) collective-permute-start(bf16[1,2,2,192,1024]{4,3,2,1,0:T(8,128)(2,1)} %bitcast.21), channel_id=1, source_target_pairs={{0,1},{1,0},{2,3},{3,2},{4,5},{5,4},{6,7},{7,6},{8,9},{9,8},{10,11... | collective-permute-start | bytes 4718600 | tf_op jit(solution)/shard_map/ppermute | solution.py:120
  289.0 3.8 %collective-permute-start.15 = (bf16[1,2,2,192,1024]{4,3,2,1,0:T(8,128)(2,1)S(1)}, bf16[1,2,2,192,1024]{4,3,2,1,0:T(8,128)(2,1)S(1)}, u32[]{:S(2)}, u32[]{:S(2)}) collective-permute-start(bf16[1,2,2,192,1024]{4,3,2,1,0:T(8,128)(2,1)S(1)} %bitcast.85), channel_id=1, source_target_pairs={{0,1},{1,0},{2,3},{3,2},{4,5},{5,4},{6,7},{7,6},{8,9},{9,8},{10,11... | collective-permute-start | bytes 4718600 | tf_op jit(solution)/shard_map/ppermute | solution.py:120
  291.2 20.0 %collective-permute-start.13 = (bf16[1,1,2,192,1024]{4,3,2,1,0:T(8,128)(2,1)S(1)}, bf16[1,1,2,192,1024]{4,3,2,1,0:T(8,128)(2,1)S(1)}, u32[]{:S(2)}, u32[]{:S(2)}) collective-permute-start(bf16[1,1,2,192,1024]{4,3,2,1,0:T(8,128)(2,1)S(1)} %slice.153), channel_id=1, source_target_pairs={{0,2},{1,3},{2,0},{3,1},{4,6},{5,7},{6,4},{7,5},{8,10},{9,11},{10,... | collective-permute-start | bytes 2359304 | tf_op jit(solution)/shard_map/ppermute | solution.py:120
  293.5 19.7 %collective-permute-start.16 = (bf16[1,2,1,192,1024]{4,3,2,1,0:T(8,128)(2,1)S(1)}, bf16[1,2,1,192,1024]{4,3,2,1,0:T(8,128)(2,1)S(1)}, u32[]{:S(2)}, u32[]{:S(2)}) collective-permute-start(bf16[1,2,1,192,1024]{4,3,2,1,0:T(8,128)(2,1)S(1)} %slice.160), channel_id=1, source_target_pairs={{0,4},{4,0},{1,5},{5,1},{2,6},{6,2},{3,7},{7,3},{8,12},{12,8},{9,1... | collective-permute-start | bytes 2359304 | tf_op jit(solution)/shard_map/ppermute | solution.py:120
  311.6 10.7 %collective-permute-start.14 = (bf16[1,1,1,192,1024]{4,3,2,1,0:T(8,128)(2,1)S(1)}, bf16[1,1,1,192,1024]{4,3,2,1,0:T(8,128)(2,1)S(1)}, u32[]{:S(2)}, u32[]{:S(2)}) collective-permute-start(bf16[1,1,1,192,1024]{4,3,2,1,0:T(8,128)(2,1)S(1)} %slice.155), channel_id=1, source_target_pairs={{0,4},{4,0},{1,5},{5,1},{2,6},{6,2},{3,7},{7,3},{8,12},{12,8},{9,1... | collective-permute-start | bytes 1179656 | tf_op jit(solution)/shard_map/ppermute | solution.py:120
  313.6 10.4 %collective-permute-start.17 = (bf16[1,1,1,192,1024]{4,3,2,1,0:T(8,128)(2,1)S(1)}, bf16[1,1,1,192,1024]{4,3,2,1,0:T(8,128)(2,1)S(1)}, u32[]{:S(2)}, u32[]{:S(2)}) collective-permute-start(bf16[1,1,1,192,1024]{4,3,2,1,0:T(8,128)(2,1)S(1)} %slice.162), channel_id=1, source_target_pairs={{0,2},{1,3},{2,0},{3,1},{4,6},{5,7},{6,4},{7,5},{8,10},{9,11},{10,... | collective-permute-start | bytes 1179656 | tf_op jit(solution)/shard_map/ppermute | solution.py:120
Sparse Core Ops, SparseCore 0:
  20.9 36.5 all-gather.5
  59.1 62.2 all-gather.7
  122.9 56.6 all-gather.9
  181.1 67.6 all-gather.11
  250.2 33.7 all-gather.13
